TPU v7x, 32 devices: a whole 2x2x4 slice. The times are simulated.
32 devices in a mesh: sp: 4 (over z), fs: 4 (over y, x), tp: 2 (over core).
Axes of the slice: x: 2, y: 2, z: 4, core: 2. Of those that a mesh axis runs over, the one named last changes fastest.
Arguments:
- tokens: bfloat16 [4, 2048, 2048], P('fs', 'sp', 'tp'), may hold values from -6 to 6
- norm_gain: float32 [2048], replicated, may hold values from 0.1 to 1.9
- query_weight: bfloat16 [2048, 1024], P(('sp', 'fs'), 'tp'), may hold values from -0.125 to 0.125
- key_weight: bfloat16 [2048, 1024], P(('sp', 'fs'), 'tp'), may hold values from -0.125 to 0.125
- value_weight: bfloat16 [2048, 2048], P(('sp', 'fs'), 'tp'), may hold values from -0.125 to 0.125
- outgate_weight: bfloat16 [2048, 2048], P(('sp', 'fs'), 'tp'), may hold values from -0.125 to 0.125
- gate_weight: bfloat16 [2048, 2, 16], P(('sp', 'fs'), None, 'tp'), may hold values from -6 to 6
- forget_bias: float32 [16], P('tp')
- forget_shift: float32 [4, 16, 2048], P('fs', 'tp', 'sp'), may hold values from -1.5 to 0
- head_norm_gain: float32 [2048], P('tp'), may hold values from 0.1 to 1.9
- exit_weight: bfloat16 [2048, 2048], P(('sp', 'fs'), 'tp'), may hold values from -0.125 to 0.125
- entry_weight: bfloat16 [2048, 2048], P(('sp', 'fs'), 'tp'), may hold values from -0.125 to 0.125
- signal_weight: bfloat16 [2048, 2048], P(('sp', 'fs'), 'tp'), may hold values from -0.125 to 0.125
- conv_kernel: float32 [3, 2048], P(None, 'tp'), may hold values from -3.5 to 3.5
- merge_weight: bfloat16 [4096, 2048], P(('sp', 'fs'), 'tp'), may hold values from -0.09375 to 0.09375
Outputs:
- mixed: bfloat16 [4, 2048, 2048], P('fs', 'sp', 'tp')
All inputs are finite; a program needn't handle non-finite values.
Results may differ from a plain program's by a relative error of at most 0.017.
The roundings to bfloat16 on the way count: a program that leaves them out, or rounds other values in their place, can miss the bound.
Values may be sent and summed in bfloat16 or wider, within the bound.
A program may use at most 128 MiB of HBM per device.

v0:
```python
import jax
import jax.numpy as jnp
from jax import lax
from jax.sharding import PartitionSpec as P

DK = 64
DV = 128
BLOCK = 128
KERNEL = 3
EPSILON = 1e-06
EMPTY_LOG = -1e30
HIGHEST = lax.Precision.HIGHEST


def prefix(part, axis, combine, identity):
    place = lax.axis_index(axis)
    gathered = jax.tree.map(lambda a: lax.all_gather(a, axis), part)
    state = jax.tree.map(lambda a, e: jnp.zeros_like(a) + jnp.asarray(e, a.dtype), part, identity)

    def one(step, state):
        return combine(
            state, jax.tree.map(lambda a: lax.dynamic_index_in_dim(a, step, 0, False), gathered)
        )

    return lax.fori_loop(0, place, one, state)


def passed_along(value, axis, steps):
    count = lax.axis_size(axis)
    initial, last = (max(0, -steps), min(count, count - steps))
    return lax.ppermute(value, axis, [(source, source + steps) for source in range(initial, last)])


def combine(earlier, later):
    ceiling = jnp.maximum(later[2] + earlier[1], later[1])
    kept = jnp.exp(later[2] + earlier[1] - ceiling)
    added = jnp.exp(later[1] - ceiling)
    state = kept[..., None, None] * earlier[0] + added[..., None, None] * later[0]
    return (state, ceiling, earlier[2] + later[2])


def identity_state(heads):
    return (
        jnp.zeros((heads, DK, DV), jnp.float32),
        jnp.full((heads,), EMPTY_LOG, jnp.float32),
        jnp.zeros((heads,), jnp.float32),
    )


def add_product(left, piece):
    return jnp.dot(left, piece, preferred_element_type=jnp.float32)


def split_columns(total, stack):
    outputs = []
    offset = 0
    for weight in stack:
        outputs.append(total[:, offset : offset + weight.shape[1]])
        offset = offset + weight.shape[1]
    return outputs


def incoming_state(running):
    heads = running[1].shape[0]
    before = prefix((running[0], running[1], running[2]), "sp", combine, identity_state(heads))
    ceiling = jnp.maximum(before[1], before[2])
    shrink = jnp.exp(before[1] - ceiling)
    return (before[0] * shrink[:, None, None], ceiling, before[2])


def memory_states(keys, values, gates, forget_bias, forget_shift):
    count = gates.shape[0]
    heads = forget_bias.shape[0]
    blocks = count // BLOCK
    inputs = gates[:, :heads].reshape(blocks, BLOCK, heads)
    logs = jax.nn.log_sigmoid(gates[:, heads:] + forget_bias) + forget_shift[0].T
    cumulative = jnp.cumsum(logs.reshape(blocks, BLOCK, heads), axis=1)
    last = cumulative[:, -1]
    weight_logs = last[:, None, :] - cumulative + inputs
    peak = jnp.max(weight_logs, axis=1)
    coefficient_array = jnp.exp(weight_logs - peak[:, None, :])
    scaled = keys.reshape(blocks, BLOCK, heads, DK).astype(jnp.float32) * DK ** (-0.5)
    value_float = values.reshape(blocks, BLOCK, heads, DV).astype(jnp.float32)
    states = jnp.einsum(
        "csh,cshk,cshv->chkv", coefficient_array, scaled, value_float, precision=HIGHEST
    )
    running = identity_state(heads)
    prefixes = []
    for index in range(blocks):
        prefixes.append(running)
        running = combine(running, (states[index], peak[index], last[index]))
    leading_part = tuple((jnp.stack([item[member] for item in prefixes]) for member in range(3)))
    gate_apertures = combine(incoming_state(running), leading_part)
    return (gate_apertures, cumulative, inputs)


def memory_output(
    queries, keys, values, outgates, inputs, cumulative, gate_apertures, head_norm_gain
):
    blocks = cumulative.shape[0]
    heads = cumulative.shape[2]
    count = queries.shape[0]
    query_blocks = queries.reshape(blocks, BLOCK, heads, DK)
    key_blocks = keys.reshape(blocks, BLOCK, heads, DK)
    value_blocks = values.reshape(blocks, BLOCK, heads, DV)
    score_matrix = jnp.einsum(
        "cjhk,cshk->chjs", query_blocks, key_blocks, preferred_element_type=jnp.float32
    ) * DK ** (-0.5)
    cum_lanes = cumulative.transpose(0, 2, 1)
    input_lanes = inputs.transpose(0, 2, 1)
    causal = jnp.tril(jnp.ones((BLOCK, BLOCK), dtype=bool))
    decay = jnp.where(
        causal,
        cum_lanes[..., :, None] - cum_lanes[..., None, :] + input_lanes[..., None, :],
        -jnp.inf,
    )
    inter = cum_lanes + gate_apertures[1][..., None]
    ceiling = jnp.maximum(inter, jnp.max(decay, axis=-1))
    weighted = score_matrix * jnp.exp(decay - ceiling[..., None])
    numerator = jnp.einsum(
        "chjs,cshv->chjv",
        weighted.astype(jnp.bfloat16),
        value_blocks,
        preferred_element_type=jnp.float32,
    )
    query_float = query_blocks.astype(jnp.float32)
    carried = jnp.exp(inter - ceiling)
    numerator = numerator + carried[..., None] * jnp.einsum(
        "cjhk,chkv->chjv", query_float, gate_apertures[0], precision=HIGHEST
    )
    result = numerator * lax.rsqrt(
        jnp.mean(numerator * numerator, axis=-1, keepdims=True) + EPSILON
    )
    result = result.transpose(0, 2, 1, 3).reshape(count, heads * DV) * head_norm_gain
    return (result * jax.nn.sigmoid(outgates.astype(jnp.float32))).astype(jnp.bfloat16)


def local(
    tokens,
    norm_gain,
    query_weight,
    key_weight,
    value_weight,
    outgate_weight,
    gate_weight,
    forget_bias,
    forget_shift,
    head_norm_gain,
    exit_weight,
    entry_weight,
    signal_weight,
    conv_kernel,
    merge_weight,
):
    whole = lax.all_gather(tokens, "tp", axis=2, tiled=True)[0]
    count = whole.shape[0]
    flat = whole.astype(jnp.float32)
    normed = (
        flat * lax.rsqrt(jnp.mean(flat * flat, axis=-1, keepdims=True) + EPSILON) * norm_gain
    ).astype(jnp.bfloat16)
    gate_rows = gate_weight.reshape(gate_weight.shape[0], -1)
    state_stack = [key_weight, value_weight, gate_rows]
    other_stack = [query_weight, outgate_weight, exit_weight, entry_weight, signal_weight]
    stacked = jnp.concatenate(state_stack + other_stack, axis=1)
    total = add_product(normed, lax.all_gather(stacked, ("sp", "fs"), axis=0, tiled=True))
    columns = split_columns(total, state_stack + other_stack)
    keys = columns[0].astype(jnp.bfloat16)
    values = columns[1].astype(jnp.bfloat16)
    gate_apertures, cumulative, inputs = memory_states(
        keys, values, columns[2], forget_bias, forget_shift
    )
    others = columns[3:]
    queries = others[0].astype(jnp.bfloat16)
    outgates = others[1].astype(jnp.bfloat16)
    exit_rows = others[2].astype(jnp.bfloat16)
    entry_rows = others[3].astype(jnp.bfloat16)
    signal_rows = others[4].astype(jnp.bfloat16)
    mixed_in = (entry_rows.astype(jnp.float32) * signal_rows.astype(jnp.float32)).astype(
        jnp.bfloat16
    )
    rim = passed_along(mixed_in[count - (KERNEL - 1) :], "sp", 1)
    padded = jnp.concatenate([rim, mixed_in], axis=0).astype(jnp.float32)
    response = conv_kernel[0] * padded[0:count]
    for tap in range(1, KERNEL):
        response = response + conv_kernel[tap] * padded[tap : tap + count]
    conv_out = (exit_rows.astype(jnp.float32) * response).astype(jnp.bfloat16)
    memory_out = memory_output(
        queries, keys, values, outgates, inputs, cumulative, gate_apertures, head_norm_gain
    )
    memory_all, conv_all = (
        lax.all_gather(memory_out, "tp", axis=1, tiled=True),
        lax.all_gather(conv_out, "tp", axis=1, tiled=True),
    )
    concatenated_result = jnp.concatenate([memory_all, conv_all], axis=1)
    mixed = add_product(
        concatenated_result, lax.all_gather(merge_weight, ("sp", "fs"), axis=0, tiled=True)
    )
    return mixed.astype(jnp.bfloat16)[None]


def whole_states(keys, values, inputs, logs, blocks):
    heads = inputs.shape[1]
    inputs = inputs.reshape(blocks, BLOCK, heads)
    upto = jnp.tril(jnp.ones((BLOCK, BLOCK), jnp.float32))
    cumulative = jnp.einsum(
        "js,csh->cjh", upto, logs.reshape(blocks, BLOCK, heads), precision=HIGHEST
    )
    last = cumulative[:, -1]
    weight_logs = last[:, None, :] - cumulative + inputs
    peak = jnp.max(weight_logs, axis=1)
    coefficients = jnp.exp(weight_logs - peak[:, None, :])
    scaled = keys.reshape(blocks, BLOCK, heads, DK).astype(jnp.float32) * DK ** (-0.5)
    weighted_keys = scaled * coefficients[..., None]
    value_float = values.reshape(blocks, BLOCK, heads, DV).astype(jnp.float32)
    states = jnp.einsum("cshk,cshv->chkv", weighted_keys, value_float, precision=HIGHEST)
    place = jnp.arange(blocks)
    between = (place[None, :, None] < place[None, None, :]) & (
        place[None, None, :] < place[:, None, None]
    )
    decay = jnp.sum(jnp.where(between[..., None], last[None, None], 0.0), axis=2) + peak[None]
    earlier = (place[None, :] < place[:, None])[..., None]
    decay = jnp.where(earlier, decay, -jnp.inf)
    start = jnp.sum(jnp.where(earlier, last[None], 0.0), axis=1)
    ceiling = jnp.maximum(start, jnp.max(decay, axis=1))
    shares = jnp.exp(decay - ceiling[:, None])
    before = jnp.einsum("cdh,dhkv->chkv", shares, states, precision=HIGHEST)
    return ((before, ceiling), cumulative, inputs)


def resharded(
    tokens,
    norm_gain,
    query_weight,
    key_weight,
    value_weight,
    outgate_weight,
    gate_weight,
    forget_bias,
    forget_shift,
    head_norm_gain,
    exit_weight,
    entry_weight,
    signal_weight,
    conv_kernel,
    merge_weight,
):
    parts = lax.axis_size("sp")
    place = lax.axis_index("sp")
    depth = key_weight.shape[0]
    gates = gate_weight.shape[2]
    heads = gates // parts
    stack = [
        query_weight,
        key_weight,
        value_weight,
        outgate_weight,
        exit_weight,
        entry_weight,
        signal_weight,
        gate_weight.reshape(depth, 2, parts, heads).transpose(0, 2, 1, 3),
    ]
    stacked = jnp.concatenate([w.reshape(depth, parts, -1) for w in stack], axis=2)
    widths = [w.size // depth // parts for w in stack]
    sent = lax.all_to_all(stacked.transpose(1, 0, 2), "sp", 0, 0)
    rows = lax.all_gather(sent, "fs", axis=1)
    rows = rows.reshape(-1, rows.shape[-1])
    line = lax.all_gather(tokens[0], "sp", axis=0, tiled=True)
    whole = lax.all_gather(line, "tp", axis=1, tiled=True)
    count = whole.shape[0]
    flat = whole.astype(jnp.float32)
    normed = (
        flat * lax.rsqrt(jnp.mean(flat * flat, axis=-1, keepdims=True) + EPSILON) * norm_gain
    ).astype(jnp.bfloat16)
    total = add_product(normed, rows)
    columns = []
    offset = 0
    for width in widths:
        columns.append(total[:, offset : offset + width])
        offset = offset + width
    queries, keys, values, outgates, exit_rows, entry_rows, signal_rows = [
        c.astype(jnp.bfloat16) for c in columns[:7]
    ]
    gate_pre = columns[7]

    def own(array, axis, width):
        return lax.dynamic_slice_in_dim(array, place * width, width, axis)

    shift = lax.all_to_all(forget_shift[0].reshape(parts, heads, -1), "sp", 0, 0)
    shift = shift.transpose(1, 0, 2).reshape(heads, count)
    logs = jax.nn.log_sigmoid(gate_pre[:, heads:] + own(forget_bias, 0, heads)) + shift.T
    blocks = count // BLOCK
    apertures, cumulative, inputs = whole_states(keys, values, gate_pre[:, :heads], logs, blocks)
    channels = exit_rows.shape[1]
    taps = own(conv_kernel, 1, channels)
    mixed_in = (entry_rows.astype(jnp.float32) * signal_rows.astype(jnp.float32)).astype(
        jnp.bfloat16
    )
    padded = jnp.pad(mixed_in, ((KERNEL - 1, 0), (0, 0))).astype(jnp.float32)
    response = taps[0] * padded[0:count]
    for tap in range(1, KERNEL):
        response = response + taps[tap] * padded[tap : tap + count]
    conv_out = (exit_rows.astype(jnp.float32) * response).astype(jnp.bfloat16)
    memory_out = memory_output(
        queries,
        keys,
        values,
        outgates,
        inputs,
        cumulative,
        apertures,
        own(head_norm_gain, 0, heads * DV),
    )
    both = jnp.concatenate([memory_out, conv_out], axis=1)
    back = lax.all_to_all(both.reshape(parts, count // parts, -1), "sp", 0, 0)
    halves = lax.all_gather(back, "tp")
    memory_width = heads * DV
    memory_all = halves[..., :memory_width].transpose(2, 0, 1, 3).reshape(count // parts, -1)
    conv_all = halves[..., memory_width:].transpose(2, 0, 1, 3).reshape(count // parts, -1)
    merge = lax.all_gather(merge_weight, ("sp", "fs"), axis=0, tiled=True)
    mixed = add_product(jnp.concatenate([memory_all, conv_all], axis=1), merge)
    return mixed.astype(jnp.bfloat16)[None]


def solution(mesh):
    placed = (
        P("fs", "sp", "tp"),
        P(),
        P(("sp", "fs"), "tp"),
        P(("sp", "fs"), "tp"),
        P(("sp", "fs"), "tp"),
        P(("sp", "fs"), "tp"),
        P(("sp", "fs"), None, "tp"),
        P("tp"),
        P("fs", "tp", "sp"),
        P("tp"),
        P(("sp", "fs"), "tp"),
        P(("sp", "fs"), "tp"),
        P(("sp", "fs"), "tp"),
        P(None, "tp"),
        P(("sp", "fs"), "tp"),
    )
    sp, tp = (mesh.shape["sp"], mesh.shape["tp"])

    def step(*args):
        heads, channels = (args[6].shape[2], args[10].shape[1])
        even = heads % (sp * tp) == 0 and channels % (sp * tp * 128) == 0
        body = resharded if even else local
        return jax.shard_map(
            body, mesh=mesh, in_specs=placed, out_specs=P("fs", "sp", "tp"), check_vma=False
        )(*args)

    return step
```

profile of v0, /device:TPU:0, one launch (start us, length us, event | category | flops | bytes accessed | tf_op | source)
XLA Modules:
  0.0 471.0 jit_solution(17754036155125778785)
XLA Ops:
  6.6 0.7 all-gather.12.cloned.1.call-update
  7.3 1.0 copy.151
  8.3 1.0 copy.152
  9.4 1.1 copy.153
  10.5 0.2 copy.154
  10.7 0.2 copy.155
  10.9 0.2 copy.156
  11.1 0.2 copy.157
  11.6 85.0 %all_to_all.15 = bf16[4,128,1540]{1,2,0:T(8,128)(2,1)} all-to-all(bf16[4,128,1540]{1,2,0:T(8,128)(2,1)S(1)} %bitcast.143), channel_id=1, replica_groups=mesh['sp'=4,'fs'=4,'tp'=2] {'sp'}, dimensions={0} | all-to-all | bytes 3153920 | tf_op jit(solution)/shard_map/all_to_all | solution.py:264
  96.5 0.0 all-gather.14.cloned.1.call-start
  96.6 26.0 %all-gather.12.cloned.1.call-done = bf16[1,2048,1024]{2,1,0:T(8,128)(2,1)} async-done(((bf16[1,512,1024]{2,1,0:T(8,128)(2,1)}), bf16[1,2048,1024]{2,1,0:T(8,128)(2,1)}) %all-gather.12.cloned.1.call-update) | async-done | bytes 4194320 | tf_op jit(solution)/shard_map/all_gather | solution.py:267
  122.6 0.7 copy-done.7
  123.3 0.6 reshape_squeeze.3
  123.9 3.3 all-to-all-start.1
  127.2 0.0 all-gather.18.cloned.1.call-start
  127.3 0.1 dynamic_slice.9
  127.3 0.8 dynamic_slice.10
  128.1 0.9 constant_dynamic-slice_fusion
  129.0 64.8 %all-gather.16.cloned.1.call-done = bf16[4,512,1540]{1,2,0:T(8,128)(2,1)} async-done(((bf16[4,128,1540]{1,2,0:T(8,128)(2,1)}), bf16[4,512,1540]{1,2,0:T(8,128)(2,1)}) %all-gather.16.cloned.1.call-update) | async-done | bytes 6307856 | tf_op jit(solution)/shard_map/all_gather | solution.py:265
  193.9 17.7 %copy.243 = bf16[4,512,1540]{1,0,2:T(4,128)(2,1)S(1)} copy(bf16[4,512,1540]{1,2,0:T(8,128)(2,1)} %all-gather.16.cloned.1.call-done) | data formatting | bytes 12615680 | tf_op jit(solution)/shard_map/all_gather | solution.py:265
  211.6 2.6 pad.9
  214.2 5.3 %copy.191 = bf16[193,8,4,512]{3,1,2,0:T(8,128)(2,1)} copy(bf16[193,8,4,512]{3,2,1,0:T(4,128)(2,1)S(1)} %bitcast.129) | data formatting | bytes 12648448
  219.5 5.2 %fusion = f32[2048]{0:T(1024)S(1)} fusion(bf16[1,2048,2048]{2,1,0:T(8,128)(2,1)} %all-gather.14.cloned.1.call-done), kind=kLoop, calls=%fused_computation.2 | loop fusion | flops 12580864 | bytes 8396800 | tf_op jit(solution)/shard_map/reduce_sum | solution.py:272
  224.8 0.5 copy-done
  225.3 18.9 %fusion.78 = (bf16[2048,1540]{0,1:T(8,128)(2,1)}, f32[2048,1540]{0,1:T(8,128)}) fusion(bf16[2048,1540]{0,1:T(8,128)(2,1)} %bitcast.135, bf16[1,2048,2048]{2,1,0:T(8,128)(2,1)S(1)} %copy-done, f32[2048]{0:T(1024)S(1)} %copy-done.9, f32[2048]{0:T(1024)S(1)} %add_rsqrt_fusion), kind=kOutput, calls=%fused_computation.117 | convolution fusion | flops 12938387456 | bytes 33636352 | tf_op jit(solution)/shard_map/dot_general | solution.py:51
  244.1 1.0 fusion.56
  245.2 0.2 fusion.48
  245.4 0.2 slice_reduce_fusion
  245.6 0.2 fusion.70
  245.7 0.2 select_reduce_fusion
  245.9 0.1 fusion.65
  246.0 0.1 copy.188
  246.1 0.1 copy.189
  246.2 0.1 copy.168
  246.3 1.3 fusion.20
  247.6 0.1 subtract_exponential_fusion
  247.7 0.1 fusion.53
  247.8 1.3 slice_bitcast_fusion.2
  249.1 1.3 slice_bitcast_fusion
  250.4 0.1 copy.193
  250.6 0.2 copy.196
  250.8 0.9 copy.177
  251.7 1.0 fusion.31
  252.7 1.6 convolution_bitcast_fusion
  254.3 0.1 copy.192
  254.5 0.8 copy-done.2
  255.3 1.9 fusion.28
  257.2 4.6 multiply_reduce_fusion
  261.8 2.1 fusion.19
  264.0 1.2 copy.183
  265.2 3.3 fusion.13
  268.5 0.4 pad_convert_fusion
  268.9 2.7 fusion.16
  271.6 0.1 pad_maximum_fusion
  271.7 0.4 copy.244
  272.1 52.4 %all_to_all.16 = bf16[4,512,512]{1,2,0:T(8,128)(2,1)S(1)} all-to-all(bf16[4,512,512]{1,2,0:T(8,128)(2,1)S(1)} %bitcast.133), channel_id=1, replica_groups=mesh['sp'=4,'fs'=4,'tp'=2] {'sp'}, dimensions={0} | all-to-all | bytes 4194304 | tf_op jit(solution)/shard_map/all_to_all | solution.py:314
  324.5 2.4 copy.185
  326.9 0.0 all-gather.10.cloned.1.call-start
  327.0 0.5 all-gather.10.cloned.1.call-update
  327.5 11.4 %all-gather.18.cloned.1.call-done = bf16[8,512,512]{2,1,0:T(8,128)(2,1)} async-done(((bf16[4,512,512]{2,1,0:T(8,128)(2,1)}), bf16[8,512,512]{2,1,0:T(8,128)(2,1)}) %all-gather.18.cloned.1.call-update) | async-done | bytes 4194320 | tf_op jit(solution)/shard_map/all_gather | solution.py:315
  338.9 6.4 %copy.186 = bf16[8,512,512]{1,2,0:T(8,128)(2,1)} copy(bf16[8,512,512]{2,1,0:T(8,128)(2,1)} %all-gather.18.cloned.1.call-done) | data formatting | bytes 8388608 | tf_op jit(solution)/shard_map/all_gather | solution.py:315
  345.3 4.0 fusion.77
  349.3 105.7 %all-gather.10.cloned.1.call-done = bf16[4096,1024]{1,0:T(8,128)(2,1)} async-done(((bf16[256,1024]{1,0:T(8,128)(2,1)}), bf16[4096,1024]{1,0:T(8,128)(2,1)}) %all-gather.10.cloned.1.call-update) | async-done | bytes 8388624 | tf_op jit(solution)/shard_map/all_gather | solution.py:319
  455.0 9.5 %fusion.25 = bf16[1,512,1024]{2,1,0:T(8,128)(2,1)} fusion(bf16[4096,1024]{1,0:T(8,128)(2,1)} %all-gather.10.cloned.1.call-done, bf16[512,2048]{0,1:T(8,128)(2,1)} %bitcast.142, bf16[512,2048]{0,1:T(8,128)(2,1)S(1)} %bitcast.141), kind=kOutput, calls=%fused_computation.36 | convolution fusion | flops 4303880192 | bytes 13631488 | tf_op jit(solution)/shard_map/dot_general | solution.py:51
  (48 shorter events, 0.6 us)
Async XLA Ops:
  6.5 4.0 copy-start.3
  6.5 4.2 copy-start.4
  6.5 4.3 copy-start.5
  6.5 4.5 copy-start.6
  6.5 116.0 %all-gather.12.cloned.1.call-start = ((), (), s32[]{:S(2)}) async-start(), calls=%async_computation.4 | async-start | bytes 5242880 | tf_op jit(solution)/shard_map/all_gather | solution.py:267
  6.6 4.7 copy-start.8
  7.3 186.6 %all-gather.16.cloned.1.call-start = ((), (), s32[]{:S(2)}) async-start(), calls=%async_computation.6 | async-start | bytes 7905280 | tf_op jit(solution)/shard_map/all_gather | solution.py:265
  96.5 123.0 %all-gather.14.cloned.1.call-start = ((), (), s32[]{:S(2)}) async-start(), calls=%async_computation.5 | async-start | bytes 12582912 | tf_op jit(solution)/shard_map/all_gather | solution.py:268
  122.6 0.7 copy-start.7
  122.6 4.7 copy-start.10
  123.9 120.2 %all-to-all-start.1 = ((f32[4,2,512]{2,1,0:T(2,128)}), f32[4,2,512]{2,1,0:T(2,128)S(1)}, u32[]{:S(2)}, u32[]{:S(2)}) async-start(f32[4,2,512]{2,1,0:T(2,128)} %reshape_squeeze.3), calls=%async_computation.1 | async-start | bytes 32768 | tf_op jit(solution)/shard_map/all_to_all | solution.py:288
  127.2 211.7 %all-gather.18.cloned.1.call-start = ((), (), s32[]{:S(2)}) async-start(), calls=%async_computation.7 | async-start | bytes 6291456 | tf_op jit(solution)/shard_map/all_gather | solution.py:315
  219.5 5.3 %copy-start.9 = (f32[2048]{0:T(1024)S(1)}, f32[2048]{0:T(1024)}, u32[]{:S(2)}) copy-start(f32[2048]{0:T(1024)} %param.16) | copy-start | bytes 24580
  219.5 5.8 %copy-start = (bf16[1,2048,2048]{2,1,0:T(8,128)(2,1)S(1)}, bf16[1,2048,2048]{2,1,0:T(8,128)(2,1)}, u32[]{:S(2)}) copy-start(bf16[1,2048,2048]{2,1,0:T(8,128)(2,1)} %all-gather.14.cloned.1.call-done) | copy-start | bytes 25165828
  250.6 1.2 copy-start.1
  254.4 0.8 copy-start.2
  326.9 128.1 %all-gather.10.cloned.1.call-start = ((), (), s32[]{:S(2)}) async-start(), calls=%async_computation.3 | async-start | bytes 8912896 | tf_op jit(solution)/shard_map/all_gather | solution.py:319
Sparse Core Ops, SparseCore 0:
  8.9 113.6 all-gather.11
  124.4 69.3 all-gather.15
  195.4 19.8 all-gather.13
  327.0 11.7 all-gather.17
  341.5 113.4 all-gather.9
where the time goes:
time: 472 us; the launch traced here: 471 us
  waiting for transfers between devices  209 us (44%)
  blocking collectives  137 us (29%)
  local copies, waits for them, and re-layouts  52.9 us (11%)
  matrix products  37.7 us (8%)
  other arithmetic  16.9 us (4%)
  between operations  13.6 us (3%)
    all_gather x1, waiting for transfers between devices, resharded(): merge = lax.all_gather(merge_weight, ('sp', 'fs'), axis=0, tiled=True)  106 us
    all_to_all x1, blocking collectives, resharded(): sent = lax.all_to_all(stacked.transpose(1, 0, 2), 'sp', 0, 0)  85 us
    all_gather x1, waiting for transfers between devices, resharded(): rows = lax.all_gather(sent, 'fs', axis=1)  64.8 us
    all_to_all x1, blocking collectives, resharded(): back = lax.all_to_all(both.reshape(parts, count // parts, -1), 'sp', 0, 0)  52.4 us
    dot_general x2, matrix products, add_product(): return jnp.dot(left, piece, preferred_element_type=jnp.float32)  28.4 us
    all_gather x1, waiting for transfers between devices, resharded(): line = lax.all_gather(tokens[0], 'sp', axis=0, tiled=True)  26 us
    all_gather x1, local copies, waits for them, and re-layouts, resharded(): rows = lax.all_gather(sent, 'fs', axis=1)  17.7 us
    unnamed x46, local copies, waits for them, and re-layouts  17.2 us
  transfers between devices with their start and end apart: 6, of which 4 were waited for; matrix products, arithmetic and copies ran while one was open for 14% of the time, Pallas kernels for 0%

commit v1 on v0

--- a/solution.py
+++ b/solution.py
@@ -265,7 +265,8 @@
     rows = lax.all_gather(sent, "fs", axis=1)
     rows = rows.reshape(-1, rows.shape[-1])
     line = lax.all_gather(tokens[0], "sp", axis=0, tiled=True)
-    whole = lax.all_gather(line, "tp", axis=1, tiled=True)
+    block_next = jax.lax.all_gather(line, axis_name="tp")
+    whole = jnp.concatenate(block_next, axis=1)
     count = whole.shape[0]
     flat = whole.astype(jnp.float32)
     normed = (

time: 472 us -> 494 us (1.047)
  local copies, waits for them, and re-layouts: 52.9 us -> 64.4 us
  other arithmetic: 16.9 us -> 25.3 us
    all_gather x0 -> x1, local copies, waits for them, and re-layouts: none -> 11.7 us  [resharded(): block_next = jax.lax.all_gather(line, axis_name='tp')]
    convert_element_type x0 -> x1, other arithmetic: none -> 8.55 us  [resharded(): normed = (flat * lax.rsqrt(jnp.mean(flat * flat, axis=-1, keepdims=True)...]
    unnamed x46 -> x44, local copies, waits for them, and re-layouts: 17.2 us -> 16.7 us
  transfers between devices with their start and end apart: 6 -> 6, of which waited for: 4 -> 4; matrix products, arithmetic and copies ran while one was open for 14% -> 18% of each run, Pallas kernels for 0% -> 0%
where the time goes in v1:
time: 494 us; the launch traced here: 492 us
  waiting for transfers between devices  209 us (42%)
  blocking collectives  137 us (28%)
  local copies, waits for them, and re-layouts  64.4 us (13%)
  matrix products  39.2 us (8%)
  other arithmetic  25.3 us (5%)
  between operations  13.6 us (3%)
    all_gather x1, waiting for transfers between devices, resharded(): merge = lax.all_gather(merge_weight, ('sp', 'fs'), axis=0, tiled=True)  106 us
    all_to_all x1, blocking collectives, resharded(): sent = lax.all_to_all(stacked.transpose(1, 0, 2), 'sp', 0, 0)  85 us
    all_gather x1, waiting for transfers between devices, resharded(): rows = lax.all_gather(sent, 'fs', axis=1)  64.8 us
    all_to_all x1, blocking collectives, resharded(): back = lax.all_to_all(both.reshape(parts, count // parts, -1), 'sp', 0, 0)  52.4 us
    dot_general x2, matrix products, add_product(): return jnp.dot(left, piece, preferred_element_type=jnp.float32)  29.9 us
    all_gather x1, waiting for transfers between devices, resharded(): line = lax.all_gather(tokens[0], 'sp', axis=0, tiled=True)  26 us
    all_gather x1, local copies, waits for them, and re-layouts, resharded(): rows = lax.all_gather(sent, 'fs', axis=1)  17.7 us
    unnamed x44, local copies, waits for them, and re-layouts  16.7 us
  transfers between devices with their start and end apart: 6, of which 4 were waited for; matrix products, arithmetic and copies ran while one was open for 18% of the time, Pallas kernels for 0%

profile of v1, /device:TPU:0, one launch (start us, length us, event | category | flops | bytes accessed | tf_op | source)
XLA Modules:
  0.0 492.5 jit_solution(5456183551933837473)
XLA Ops:
  6.6 0.7 all-gather.12.cloned.1.call-update
  7.3 1.0 copy.156
  8.3 1.0 copy.157
  9.4 1.1 copy.158
  10.5 0.2 copy.159
  10.7 0.2 copy.160
  10.9 0.2 copy.161
  11.1 0.2 copy.162
  11.6 85.0 %all_to_all.15 = bf16[4,128,1540]{1,2,0:T(8,128)(2,1)} all-to-all(bf16[4,128,1540]{1,2,0:T(8,128)(2,1)S(1)} %bitcast.139), channel_id=1, replica_groups=mesh['sp'=4,'fs'=4,'tp'=2] {'sp'}, dimensions={0} | all-to-all | bytes 3153920 | tf_op jit(solution)/shard_map/all_to_all | solution.py:264
  96.6 26.0 %all-gather.12.cloned.1.call-done = bf16[1,2048,1024]{2,1,0:T(8,128)(2,1)} async-done(((bf16[1,512,1024]{2,1,0:T(8,128)(2,1)}), bf16[1,2048,1024]{2,1,0:T(8,128)(2,1)}) %all-gather.12.cloned.1.call-update) | async-done | bytes 4194320 | tf_op jit(solution)/shard_map/all_gather | solution.py:267
  122.6 0.7 copy-done.6
  123.3 0.6 reshape_squeeze.3
  123.9 3.3 all-to-all-start.1
  127.2 0.0 all-gather.18.cloned.1.call-start
  127.3 0.1 dynamic_slice.9
  127.4 0.8 dynamic_slice.10
  128.1 0.9 constant_dynamic-slice_fusion
  129.1 64.8 %all-gather.16.cloned.1.call-done = bf16[4,512,1540]{1,2,0:T(8,128)(2,1)} async-done(((bf16[4,128,1540]{1,2,0:T(8,128)(2,1)}), bf16[4,512,1540]{1,2,0:T(8,128)(2,1)}) %all-gather.16.cloned.1.call-update) | async-done | bytes 6307856 | tf_op jit(solution)/shard_map/all_gather | solution.py:265
  193.9 17.7 %copy.248 = bf16[4,512,1540]{1,0,2:T(4,128)(2,1)S(1)} copy(bf16[4,512,1540]{1,2,0:T(8,128)(2,1)} %all-gather.16.cloned.1.call-done) | data formatting | bytes 12615680 | tf_op jit(solution)/shard_map/all_gather | solution.py:265
  211.6 2.6 pad.9
  214.2 5.4 %copy.196 = bf16[193,8,4,512]{3,1,2,0:T(8,128)(2,1)} copy(bf16[193,8,4,512]{3,2,1,0:T(4,128)(2,1)S(1)} %bitcast.124) | data formatting | bytes 12648448
  219.5 11.7 %copy.155 = bf16[2,2048,1024]{1,2,0:T(8,128)(2,1)} copy(bf16[2,2048,1024]{2,1,0:T(8,128)(2,1)} %all-gather.14.cloned.1.call-done) | data formatting | bytes 16777216 | tf_op jit(solution)/shard_map/all_gather | solution.py:268
  231.3 5.1 %fusion = f32[2048]{0:T(1024)S(1)} fusion(bf16[2,2048,1024]{1,2,0:T(8,128)(2,1)} %copy.155), kind=kLoop, calls=%fused_computation.2 | loop fusion | flops 12580864 | bytes 8396800 | tf_op jit(solution)/shard_map/reduce_sum | solution.py:273
  236.4 8.6 %fusion.2 = bf16[2,2048,1024]{1,2,0:T(8,128)(2,1)} fusion(bf16[2,2048,1024]{1,2,0:T(8,128)(2,1)} %copy.155, f32[2,1024]{1,0:T(2,128)S(1)} %mul.132, f32[2048]{0:T(1024)S(1)} %add_rsqrt_fusion), kind=kLoop, calls=%fused_computation.4 | loop fusion | flops 16777216 | bytes 16793600 | tf_op jit(solution)/shard_map/convert_element_type | solution.py:274
  244.9 20.4 %fusion.73 = (bf16[2048,1540]{0,1:T(8,128)(2,1)}, f32[2048,1540]{0,1:T(8,128)}) fusion(bf16[2048,2048]{0,1:T(8,128)(2,1)} %bitcast.127, bf16[2048,1540]{0,1:T(8,128)(2,1)} %bitcast.131), kind=kOutput, calls=%fused_computation.113 | convolution fusion | flops 12921610240 | bytes 33619968 | tf_op jit(solution)/shard_map/dot_general | solution.py:51
  265.3 1.0 fusion.51
  266.4 0.2 fusion.43
  266.6 0.2 slice_reduce_fusion
  266.8 0.2 fusion.65
  266.9 0.2 select_reduce_fusion
  267.1 0.1 fusion.60
  267.2 0.1 copy.193
  267.3 0.1 copy.194
  267.4 0.1 copy.173
  267.5 1.3 fusion.15
  268.8 0.1 subtract_exponential_fusion
  268.9 0.1 fusion.48
  269.0 1.3 slice_bitcast_fusion.2
  270.3 1.3 slice_bitcast_fusion
  271.6 0.1 copy.198
  271.8 0.2 copy.201
  272.0 1.1 copy.182
  273.1 1.0 fusion.26
  274.1 1.6 convolution_bitcast_fusion
  275.7 0.1 copy.197
  275.9 0.8 copy-done.1
  276.7 1.9 fusion.23
  278.6 4.6 multiply_reduce_fusion
  283.2 2.1 fusion.14
  285.4 1.2 copy.188
  286.6 3.3 fusion.8
  289.9 0.4 pad_convert_fusion
  290.3 2.7 fusion.11
  293.0 0.1 pad_maximum_fusion
  293.1 0.4 copy.249
  293.5 52.4 %all_to_all.16 = bf16[4,512,512]{1,2,0:T(8,128)(2,1)S(1)} all-to-all(bf16[4,512,512]{1,2,0:T(8,128)(2,1)S(1)} %bitcast.129), channel_id=1, replica_groups=mesh['sp'=4,'fs'=4,'tp'=2] {'sp'}, dimensions={0} | all-to-all | bytes 4194304 | tf_op jit(solution)/shard_map/all_to_all | solution.py:315
  346.0 2.4 copy.190
  348.4 0.0 all-gather.10.cloned.1.call-start
  348.4 0.5 all-gather.10.cloned.1.call-update
  349.0 11.4 %all-gather.18.cloned.1.call-done = bf16[8,512,512]{2,1,0:T(8,128)(2,1)} async-done(((bf16[4,512,512]{2,1,0:T(8,128)(2,1)}), bf16[8,512,512]{2,1,0:T(8,128)(2,1)}) %all-gather.18.cloned.1.call-update) | async-done | bytes 4194320 | tf_op jit(solution)/shard_map/all_gather | solution.py:316
  360.3 6.5 %copy.191 = bf16[8,512,512]{1,2,0:T(8,128)(2,1)} copy(bf16[8,512,512]{2,1,0:T(8,128)(2,1)} %all-gather.18.cloned.1.call-done) | data formatting | bytes 8388608 | tf_op jit(solution)/shard_map/all_gather | solution.py:316
  366.8 4.0 fusion.72
  370.8 105.7 %all-gather.10.cloned.1.call-done = bf16[4096,1024]{1,0:T(8,128)(2,1)} async-done(((bf16[256,1024]{1,0:T(8,128)(2,1)}), bf16[4096,1024]{1,0:T(8,128)(2,1)}) %all-gather.10.cloned.1.call-update) | async-done | bytes 8388624 | tf_op jit(solution)/shard_map/all_gather | solution.py:320
  476.4 9.5 %fusion.20 = bf16[1,512,1024]{2,1,0:T(8,128)(2,1)} fusion(bf16[4096,1024]{1,0:T(8,128)(2,1)} %all-gather.10.cloned.1.call-done, bf16[512,2048]{0,1:T(8,128)(2,1)} %bitcast.138, bf16[512,2048]{0,1:T(8,128)(2,1)S(1)} %bitcast.137), kind=kOutput, calls=%fused_computation.32 | convolution fusion | flops 4303880192 | bytes 13631488 | tf_op jit(solution)/shard_map/dot_general | solution.py:51
  (49 shorter events, 0.6 us)
Async XLA Ops:
  6.5 4.0 copy-start.2
  6.5 4.2 copy-start.3
  6.5 4.3 copy-start.4
  6.5 4.5 copy-start.5
  6.5 116.0 %all-gather.12.cloned.1.call-start = ((), (), s32[]{:S(2)}) async-start(), calls=%async_computation.4 | async-start | bytes 5242880 | tf_op jit(solution)/shard_map/all_gather | solution.py:267
  6.6 4.7 copy-start.8
  7.3 186.6 %all-gather.16.cloned.1.call-start = ((), (), s32[]{:S(2)}) async-start(), calls=%async_computation.6 | async-start | bytes 7905280 | tf_op jit(solution)/shard_map/all_gather | solution.py:265
  96.5 123.0 %all-gather.14.cloned.1.call-start = ((), (), s32[]{:S(2)}) async-start(), calls=%async_computation.5 | async-start | bytes 12582912 | tf_op jit(solution)/shard_map/all_gather | solution.py:268
  122.6 0.7 copy-start.6
  122.6 4.7 copy-start.7
  122.6 4.7 copy-start.9
  123.9 141.4 %all-to-all-start.1 = ((f32[4,2,512]{2,1,0:T(2,128)}), f32[4,2,512]{2,1,0:T(2,128)S(1)}, u32[]{:S(2)}, u32[]{:S(2)}) async-start(f32[4,2,512]{2,1,0:T(2,128)} %reshape_squeeze.3), calls=%async_computation.1 | async-start | bytes 32768 | tf_op jit(solution)/shard_map/all_to_all | solution.py:289
  127.2 233.1 %all-gather.18.cloned.1.call-start = ((), (), s32[]{:S(2)}) async-start(), calls=%async_computation.7 | async-start | bytes 6291456 | tf_op jit(solution)/shard_map/all_gather | solution.py:316
  271.8 1.4 copy-start
  275.9 0.8 copy-start.1
  348.4 128.1 %all-gather.10.cloned.1.call-start = ((), (), s32[]{:S(2)}) async-start(), calls=%async_computation.3 | async-start | bytes 8912896 | tf_op jit(solution)/shard_map/all_gather | solution.py:320
Sparse Core Ops, SparseCore 0:
  8.9 113.6 all-gather.11
  124.4 69.3 all-gather.15
  195.4 19.8 all-gather.13
  348.5 11.7 all-gather.17
  362.9 113.4 all-gather.9
